TPU v7x, 32 devices: a whole 2x2x4 slice. The times are simulated.
32 devices in a mesh: fs: 16 (over z, y, x), tp: 2 (over core).
Axes of the slice: x: 2, y: 2, z: 4, core: 2. Of those that a mesh axis runs over, the one named last changes fastest.
Arguments:
- tokens: bfloat16 [12288, 2048], P('fs'), may hold values from -6 to 6
- norm_gain: float32 [2048], replicated, may hold values from 0.1 to 1.9
- up_weight: float32 [2048, 8192], P('fs', 'tp'), may hold values from -0.125 to 0.125
- up_scale: float32 [8192], P('tp'), may hold values from 0.5 to 2
- down_weight: float32 [8192, 2048], P('tp', 'fs'), may hold values from -0.0625 to 0.0625
- down_scale: float32 [2048], P('fs'), may hold values from 0.5 to 2
Outputs:
- output: bfloat16 [12288, 2048], P('fs', 'tp')
All inputs are finite; a program needn't handle non-finite values.
Results may differ from a plain program's by a relative error of at most 0.015.
Values may be sent and summed in bfloat16 or wider, within the bound.
A program may use at most 128 MiB of HBM per device.

v0:
```python
import jax
import jax.numpy as jnp
from jax import lax
from jax.sharding import PartitionSpec as P

epsilon = 1e-06


def local(tokens, norm_gain, up_weight, up_scale, down_weight, down_scale):
    floats = tokens.astype(jnp.float32)
    inverse = lax.rsqrt(jnp.mean(floats * floats, axis=-1, keepdims=True) + epsilon)
    normed = (floats * inverse * norm_gain).astype(jnp.bfloat16)
    up_half = up_weight.astype(jnp.bfloat16)
    down_half = down_weight.astype(jnp.bfloat16)
    up_pre = jnp.dot(
        normed,
        lax.all_gather(up_half, "fs", axis=0, tiled=True),
        preferred_element_type=jnp.float32,
    )
    down_whole, scale_whole = (
        lax.all_gather(down_half, "fs", axis=1, tiled=True),
        lax.all_gather(down_scale.astype(jnp.bfloat16), "fs", axis=0, tiled=True).astype(
            down_scale.dtype
        ),
    )
    hidden = jnp.square(jax.nn.relu(up_pre * up_scale)).astype(jnp.bfloat16)
    partial_value = jnp.dot(hidden, down_whole, preferred_element_type=jnp.float32).astype(
        jnp.bfloat16
    )
    summed = lax.psum_scatter(
        partial_value.astype(jnp.float32).astype(jnp.bfloat16),
        "tp",
        scatter_dimension=1,
        tiled=True,
    ).astype(jnp.float32)
    own_width = summed.shape[1]
    own_scale = lax.dynamic_slice_in_dim(
        scale_whole, lax.axis_index("tp") * own_width, own_width, 0
    )
    return (summed * own_scale).astype(jnp.bfloat16)


def solution(mesh):
    in_specs = (P("fs", None), P(), P("fs", "tp"), P("tp"), P("tp", "fs"), P("fs"))
    out_specs = P("fs", "tp")
    return jax.shard_map(local, mesh=mesh, in_specs=in_specs, out_specs=out_specs, check_vma=False)
```

profile of v0, /device:TPU:0, one launch (start us, length us, event | category | flops | bytes accessed | tf_op | source)
XLA Modules:
  0.0 539.5 jit_solution(17070823121638339327)
XLA Ops:
  6.5 0.0 copy-start
  6.5 0.0 copy-start.1
  6.5 0.0 copy-start.2
  6.5 0.0 all-gather.6.cloned.1.call-start
  6.5 2.8 convert_element_type.36
  9.4 0.0 all-gather.6.cloned.1.call-update
  9.4 0.0 all-gather.4.cloned.1.call-start
  9.4 2.7 convert_element_type.34
  12.1 0.0 all-gather.4.cloned.1.call-update
  12.2 0.0 reduce-scatter.2.cloned.1.call-start
  12.2 0.0 copy-done
  12.2 0.7 fusion
  12.9 0.0 copy-start.3
  12.9 249.0 %all-gather.6.cloned.1.call-done = bf16[4096,2048]{1,0:T(8,128)(2,1)} async-done(((bf16[4096,128]{1,0:T(8,128)(2,1)}), bf16[4096,2048]{1,0:T(8,128)(2,1)}) %all-gather.6.cloned.1.call-update) | async-done | bytes 16777232 | tf_op jit(solution)/shard_map/all_gather | solution.py:21
  261.9 192.0 %all-gather.4.cloned.1.call-done = bf16[2048,4096]{1,0:T(8,128)(2,1)} async-done(((bf16[128,4096]{1,0:T(8,128)(2,1)}), bf16[2048,4096]{1,0:T(8,128)(2,1)}) %all-gather.4.cloned.1.call-update) | async-done | bytes 16777232 | tf_op jit(solution)/shard_map/all_gather | solution.py:17
  453.9 0.0 copy-done.1
  453.9 0.0 copy-done.2
  453.9 38.2 %convolution_convert_fusion = bf16[768,2048]{1,0:T(8,128)(2,1)} fusion(bf16[4096,2048]{1,0:T(8,128)(2,1)} %all-gather.6.cloned.1.call-done, bf16[2048,4096]{1,0:T(8,128)(2,1)} %all-gather.4.cloned.1.call-done, f32[4096]{0:T(1024)S(1)} %copy-done.1, bf16[768,2048]{1,0:T(8,128)(2,1)S(1)} %copy-done, f32[2048]{0:T(1024)S(1)} %copy-done.2, ...), kind=kOutput, calls=%fused_computation.6 | convolution fusion | flops 25790251008 | bytes 39873536 | tf_op jit(solution)/shard_map/dot_general | solution.py:27
  492.1 0.0 reduce-scatter.2.cloned.1.call-update
  492.2 0.0 copy-done.3
  492.2 37.8 %all-gather = bf16[16,1,128]{2,1,0:T(2,128)(2,1)S(1)} all-gather(bf16[1,1,128]{2,1,0:T(2,128)(2,1)S(1)} %convert_bitcast_fusion), channel_id=1, replica_groups=mesh['fs'=16,'tp'=2] {'fs'}, dimensions={0}, use_global_device_ids=true | all-gather | bytes 4352 | tf_op jit(solution)/shard_map/all_gather | solution.py:22
  530.0 0.0 reduce-scatter.2.cloned.1.call-done
  530.0 3.0 multiply_convert_fusion.1
  (4 shorter events, 0.0 us)
Async XLA Ops:
  6.5 5.7 %copy-start = (bf16[768,2048]{1,0:T(8,128)(2,1)S(1)}, bf16[768,2048]{1,0:T(8,128)(2,1)}, u32[]{:S(2)}) copy-start(bf16[768,2048]{1,0:T(8,128)(2,1)} %param.6) | copy-start | bytes 9437188
  6.5 447.4 %copy-start.1 = (f32[4096]{0:T(1024)S(1)}, f32[4096]{0:T(1024)}, u32[]{:S(2)}) copy-start(f32[4096]{0:T(1024)} %param.9) | copy-start | bytes 49156
  6.5 447.4 %copy-start.2 = (f32[2048]{0:T(1024)S(1)}, f32[2048]{0:T(1024)}, u32[]{:S(2)}) copy-start(f32[2048]{0:T(1024)} %param.7) | copy-start | bytes 24580
  6.5 255.4 %all-gather.6.cloned.1.call-start = ((), (), s32[]{:S(2)}) async-start(), calls=%async_computation.2 | async-start | bytes 17825792 | tf_op jit(solution)/shard_map/all_gather | solution.py:21
  9.4 444.5 %all-gather.4.cloned.1.call-start = ((), (), s32[]{:S(2)}) async-start(), calls=%async_computation.1 | async-start | bytes 17825792 | tf_op jit(solution)/shard_map/all_gather | solution.py:17
  12.2 517.9 %reduce-scatter.2.cloned.1.call-start = ((), (), s32[]{:S(2)}) async-start(), calls=%async_computation.3 | async-start | bytes 4718592 | tf_op jit(solution)/shard_map/reduce_scatter | solution.py:30
  12.9 479.3 %copy-start.3 = (f32[128]{0:T(128)S(1)}, f32[128]{0:T(128)}, u32[]{:S(2)}) copy-start(f32[128]{0:T(128)} %param.11) | copy-start | bytes 1540
Sparse Core Ops, SparseCore 0:
  10.0 251.8 all-gather.5
  264.7 189.1 all-gather.3
  492.3 9.1 reduce-scatter.1
where the time goes:
time: 540 us
  waiting for transfers between devices  441 us (82%)
  matrix products  38.2 us (7%)
  blocking collectives  37.8 us (7%)
  between operations  13.2 us (2%)
  other arithmetic  9.18 us (2%)
    all_gather x1, waiting for transfers between devices, local(): lax.all_gather(down_half, 'fs', axis=1, tiled=True)  249 us
    all_gather x1, waiting for transfers between devices, local(): lax.all_gather(up_half, 'fs', axis=0, tiled=True)  192 us
    dot_general x1, matrix products, local(): jnp.dot(hidden, down_whole, preferred_element_type=jnp.float32)  38.2 us
    all_gather x1, blocking collectives, local(): lax.all_gather(down_scale.astype(jnp.bfloat16), 'fs', axis=0, tiled=True)  37.8 us
  transfers between devices with their start and end apart: 3, of which 2 were waited for; matrix products, arithmetic and copies ran while one was open for 1% of the time, Pallas kernels for 0%

commit v1 on v0

--- a/solution.py
+++ b/solution.py
@@ -18,7 +18,7 @@
         preferred_element_type=jnp.float32,
     )
     down_whole, scale_whole = (
-        lax.all_gather(down_half, "fs", axis=1, tiled=True),
+        jnp.concatenate(lax.all_gather(down_half, "fs"), axis=1),
         lax.all_gather(down_scale.astype(jnp.bfloat16), "fs", axis=0, tiled=True).astype(
             down_scale.dtype
         ),

time: 540 us -> 482 us (0.89)
  waiting for transfers between devices: 441 us -> 362 us
  local copies, waits for them, and re-layouts: 0.03 us -> 21 us
    all_gather x1, waiting for transfers between devices: 249 us -> 191 us  [local(): lax.all_gather(down_half, 'fs')]
    all_gather x1, waiting for transfers between devices: 192 us -> 171 us  [local(): lax.all_gather(up_half, 'fs', axis=0, tiled=True)]
    reshape x0 -> x1, local copies, waits for them, and re-layouts: none -> 21 us  [local(): jnp.concatenate(lax.all_gather(down_half, 'fs'), axis=1)]
    dot_general x1, matrix products: 38.2 us -> 19.8 us  [local(): jnp.dot(hidden, down_whole, preferred_element_type=jnp.float32)]
    dot_general x0 -> x1, matrix products: none -> 18.5 us  [local(): jnp.dot(normed, lax.all_gather(up_half, 'fs', axis=0, tiled=True), prefer...]
  transfers between devices with their start and end apart: 3 -> 3, of which waited for: 2 -> 2; matrix products, arithmetic and copies ran while one was open for 1% -> 5% of each run, Pallas kernels for 0% -> 0%
where the time goes in v1:
time: 482 us; the launch traced here: 481 us
  waiting for transfers between devices  362 us (75%)
  matrix products  38.2 us (8%)
  blocking collectives  37.8 us (8%)
  local copies, waits for them, and re-layouts  21 us (4%)
  between operations  13.2 us (3%)
  other arithmetic  9.17 us (2%)
    all_gather x1, waiting for transfers between devices, local(): lax.all_gather(down_half, 'fs')  191 us
    all_gather x1, waiting for transfers between devices, local(): lax.all_gather(up_half, 'fs', axis=0, tiled=True)  171 us
    all_gather x1, blocking collectives, local(): lax.all_gather(down_scale.astype(jnp.bfloat16), 'fs', axis=0, tiled=True)  37.8 us
    reshape x1, local copies, waits for them, and re-layouts, local(): jnp.concatenate(lax.all_gather(down_half, 'fs'), axis=1)  21 us
    dot_general x1, matrix products, local(): jnp.dot(hidden, down_whole, preferred_element_type=jnp.float32)  19.8 us
    dot_general x1, matrix products, local(): jnp.dot(normed, lax.all_gather(up_half, 'fs', axis=0, tiled=True), prefer...  18.5 us
  transfers between devices with their start and end apart: 3, of which 2 were waited for; matrix products, arithmetic and copies ran while one was open for 5% of the time, Pallas kernels for 0%

profile of v1, /device:TPU:0, one launch (start us, length us, event | category | flops | bytes accessed | tf_op | source)
XLA Modules:
  0.0 481.4 jit_solution(6446146386558332321)
XLA Ops:
  6.5 0.0 copy-start
  6.5 0.0 all-gather.7.cloned.1.call-start
  6.5 2.8 convert_element_type.36
  9.4 0.0 all-gather.7.cloned.1.call-update
  9.4 0.0 all-gather.5.cloned.1.call-start
  9.4 2.7 convert_element_type.34
  12.1 0.0 all-gather.5.cloned.1.call-update
  12.1 0.0 reduce-scatter.2.cloned.1.call-start
  12.2 0.0 copy-done
  12.2 0.7 fusion
  12.9 191.0 %all-gather.7.cloned.1.call-done = bf16[65536,128]{1,0:T(8,128)(2,1)} async-done(((bf16[4096,128]{1,0:T(8,128)(2,1)}), bf16[65536,128]{1,0:T(8,128)(2,1)}) %all-gather.7.cloned.1.call-update) | async-done | bytes 16777232 | tf_op jit(solution)/shard_map/all_gather | solution.py:21
  203.9 0.0 copy-start.1
  203.9 0.0 copy-start.2
  203.9 21.0 %copy.8 = bf16[4096,16,128]{0,2,1:T(8,128)(2,1)} copy(bf16[4096,16,128]{2,0,1:T(8,128)(2,1)} %bitcast.22) | data formatting | bytes 33554432 | tf_op jit(solution)/shard_map/reshape | solution.py:21
  224.9 171.0 %all-gather.5.cloned.1.call-done = bf16[2048,4096]{1,0:T(8,128)(2,1)} async-done(((bf16[128,4096]{1,0:T(8,128)(2,1)}), bf16[2048,4096]{1,0:T(8,128)(2,1)}) %all-gather.5.cloned.1.call-update) | async-done | bytes 16777232 | tf_op jit(solution)/shard_map/all_gather | solution.py:17
  395.8 0.0 copy-done.1
  395.8 0.0 copy-done.2
  395.8 18.5 %fusion.26 = bf16[768,4096]{1,0:T(8,128)(2,1)} fusion(f32[4096]{0:T(1024)S(1)} %copy-done.1, bf16[2048,4096]{1,0:T(8,128)(2,1)} %all-gather.5.cloned.1.call-done, bf16[768,2048]{1,0:T(8,128)(2,1)S(1)} %copy-done, f32[2048]{0:T(1024)S(1)} %copy-done.2, f32[768]{0:T(1024)S(1)} %add_rsqrt_fusion), kind=kOutput, calls=%bitcast_fusion.clone.1 | convolution fusion | flops 12903776256 | bytes 26242048 | tf_op jit(solution)/shard_map/dot_general | solution.py:15
  414.3 19.8 %convolution_convert_fusion = bf16[768,2048]{1,0:T(8,128)(2,1)} fusion(bf16[4096,2048]{0,1:T(8,128)(2,1)} %bitcast.23, bf16[768,4096]{1,0:T(8,128)(2,1)} %fusion.26), kind=kOutput, calls=%fused_computation.6 | convolution fusion | flops 12886474752 | bytes 26214400 | tf_op jit(solution)/shard_map/dot_general | solution.py:27
  434.1 0.0 reduce-scatter.2.cloned.1.call-update
  434.1 0.0 copy-done.3
  434.1 37.8 %all-gather.1 = bf16[16,1,128]{2,1,0:T(2,128)(2,1)S(1)} all-gather(bf16[1,1,128]{2,1,0:T(2,128)(2,1)S(1)} %convert_bitcast_fusion), channel_id=1, replica_groups=mesh['fs'=16,'tp'=2] {'fs'}, dimensions={0}, use_global_device_ids=true | all-gather | bytes 4352 | tf_op jit(solution)/shard_map/all_gather | solution.py:22
  471.9 0.0 reduce-scatter.2.cloned.1.call-done
  471.9 3.0 multiply_convert_fusion.1
  (5 shorter events, 0.0 us)
Async XLA Ops:
  6.5 5.7 %copy-start = (bf16[768,2048]{1,0:T(8,128)(2,1)S(1)}, bf16[768,2048]{1,0:T(8,128)(2,1)}, u32[]{:S(2)}) copy-start(bf16[768,2048]{1,0:T(8,128)(2,1)} %param.6) | copy-start | bytes 9437188
  6.5 197.3 %all-gather.7.cloned.1.call-start = ((), (), s32[]{:S(2)}) async-start(), calls=%async_computation.3 | async-start | bytes 17825792 | tf_op jit(solution)/shard_map/all_gather | solution.py:21
  9.4 386.5 %all-gather.5.cloned.1.call-start = ((), (), s32[]{:S(2)}) async-start(), calls=%async_computation.1 | async-start | bytes 17825792 | tf_op jit(solution)/shard_map/all_gather | solution.py:17
  12.1 459.8 %reduce-scatter.2.cloned.1.call-start = ((), (), s32[]{:S(2)}) async-start(), calls=%async_computation.2 | async-start | bytes 4718592 | tf_op jit(solution)/shard_map/reduce_scatter | solution.py:30
  203.9 192.0 %copy-start.1 = (f32[4096]{0:T(1024)S(1)}, f32[4096]{0:T(1024)}, u32[]{:S(2)}) copy-start(f32[4096]{0:T(1024)} %param.9) | copy-start | bytes 49156
  203.9 192.0 %copy-start.2 = (f32[2048]{0:T(1024)S(1)}, f32[2048]{0:T(1024)}, u32[]{:S(2)}) copy-start(f32[2048]{0:T(1024)} %param.7) | copy-start | bytes 24580
  414.3 19.8 %copy-start.3 = (f32[128]{0:T(128)S(1)}, f32[128]{0:T(128)}, u32[]{:S(2)}) copy-start(f32[128]{0:T(128)} %param.11) | copy-start | bytes 1540
Sparse Core Ops, SparseCore 0:
  10.1 193.7 all-gather.6
  206.6 189.1 all-gather.4
  434.2 9.1 reduce-scatter.1
